TPU v7x, 256 devices: a whole 4x4x8 slice. The times are simulated.
256 devices in a mesh: sp: 32 (over z, y), dp: 8 (over x, core).
Axes of the slice: x: 4, y: 4, z: 8, core: 2. Of those that a mesh axis runs over, the one named last changes fastest.
Arguments:
- queries: bfloat16 [32768, 6144], P(('dp', 'sp')), may hold values from -360 to 360
- latent: bfloat16 [32768, 1024], P(('dp', 'sp')), may hold values from -6 to 6
- rope_key: bfloat16 [32768, 64], P(('dp', 'sp')), may hold values from -6 to 6
- latent_gain: float32 [1024], replicated, may hold values from 0.1 to 1.9
- kv_weight: bfloat16 [1024, 8192], P(None, 'dp'), may hold values from -0.1875 to 0.1875
- gate: bfloat16 [32768, 4096], P(('dp', 'sp')), may hold values from -6 to 6
- out_gain: float32 [4096], replicated, may hold values from 0.1 to 1.9
Outputs:
- attended: bfloat16 [32768, 4096], P(('dp', 'sp'))
All inputs are finite; a program needn't handle non-finite values.
Results may differ from a plain program's by a relative error of at most 0.007.
Values may be sent and summed in bfloat16 or wider, within the bound.
A program may use at most 128 MiB of HBM per device.

v0:
```python
import jax
import jax.numpy as jnp
from jax import lax
from jax.sharding import PartitionSpec as P

HEADS = 32
NOPE = 128
ROPE = 64
VDIM = 128
EPS = 1e-06
THETA = 10000.0


def in_order(blocks, dim):
    blocks = jnp.moveaxis(blocks, 0, dim)
    shape = blocks.shape
    return blocks.reshape(*shape[:dim], shape[dim] * shape[dim + 1], *shape[dim + 2 :])


def copy_for_each(value, axis):
    length = lax.axis_size(axis)
    return lax.all_to_all(
        jnp.broadcast_to(value[None], (length, *value.shape)), axis, 0, 0, tiled=True
    )


def gathered_copies(value, axis, dim):
    return in_order(copy_for_each(value, axis), dim)


def rotary(values, position):
    half_width = values.shape[-1] // 2
    inverse = THETA ** (-jnp.arange(half_width, dtype=jnp.float32) / half_width)
    angles = position.astype(jnp.float32)[:, None] * inverse[None, :]
    if values.ndim == 3:
        angles = angles[:, None, :]
    cosine = jnp.cos(angles)
    sine_part = jnp.sin(angles)
    front_half = values[..., :half_width].astype(jnp.float32)
    back_half = values[..., half_width:].astype(jnp.float32)
    turned = jnp.concatenate(
        [front_half * cosine - back_half * sine_part, back_half * cosine + front_half * sine_part],
        axis=-1,
    )
    return turned.astype(jnp.bfloat16)


def attend(query_block, keys_plain, keys_rotated, values):
    scores = jnp.einsum(
        "qhd,khd->hqk", query_block[..., :NOPE], keys_plain, preferred_element_type=jnp.float32
    )
    scores = scores + jnp.einsum(
        "qhr,kr->hqk", query_block[..., NOPE:], keys_rotated, preferred_element_type=jnp.float32
    )
    scores = scores * (NOPE + ROPE) ** (-0.5)
    row_max = jnp.max(scores, axis=-1, keepdims=True)
    raised = jnp.exp(scores - row_max)
    weights = (raised / jnp.sum(raised, axis=-1, keepdims=True)).astype(jnp.bfloat16)
    result = jnp.einsum("hqk,khd->qhd", weights, values, preferred_element_type=jnp.float32)
    return result.astype(jnp.bfloat16)


def per_device(queries, latent, rope_key, latent_gain, kv_weight, gate, out_gain):
    own_tokens = queries.shape[0]
    groups = lax.axis_size("sp")
    seq_len = own_tokens * groups
    offset = lax.axis_index("sp") * own_tokens
    position = offset + jnp.arange(own_tokens, dtype=jnp.int32)
    widened = latent.astype(jnp.float32)
    normed = (
        widened * lax.rsqrt(jnp.mean(widened * widened, axis=-1, keepdims=True) + EPS) * latent_gain
    ).astype(jnp.bfloat16)
    keyval = jnp.dot(
        normed,
        lax.all_gather(kv_weight, "dp", axis=1, tiled=True),
        preferred_element_type=jnp.float32,
    ).astype(jnp.bfloat16)
    head_queries = queries.reshape(own_tokens, HEADS, NOPE + ROPE)
    head_queries = jnp.concatenate(
        [head_queries[..., :NOPE], rotary(head_queries[..., NOPE:], position)], axis=-1
    )
    head_queries = head_queries.reshape(own_tokens, HEADS * (NOPE + ROPE))
    rotated_all = gathered_copies(rotary(rope_key, position), "sp", 0)
    query_all, kv_all = (
        lax.all_to_all(head_queries, "sp", split_axis=1, concat_axis=0, tiled=True),
        lax.all_to_all(keyval, "sp", split_axis=1, concat_axis=0, tiled=True),
    )
    local_heads = HEADS // groups
    rows_all = query_all.shape[0]
    seq_count = rows_all // seq_len
    block_rows = min(512, seq_len)
    block_count = seq_len // block_rows

    def one_sequence(operands):
        query_seq, kv_seq, rope_seq = operands
        keys_plain = kv_seq[..., :NOPE]
        values = kv_seq[..., NOPE:]
        blocks = query_seq.reshape(block_count, block_rows, local_heads, NOPE + ROPE)
        result = lax.map(
            lambda piece_rows: attend(piece_rows, keys_plain, rope_seq, values), blocks
        )
        return result.reshape(seq_len, local_heads * VDIM)

    heads_out = lax.map(
        one_sequence,
        (
            query_all.reshape(seq_count, seq_len, local_heads, NOPE + ROPE),
            kv_all.reshape(seq_count, seq_len, local_heads, NOPE + VDIM),
            rotated_all.reshape(seq_count, seq_len, ROPE),
        ),
    )
    heads_out = heads_out.reshape(rows_all, local_heads * VDIM)
    token_rows = lax.all_to_all(heads_out, "sp", split_axis=0, concat_axis=1, tiled=True)
    gated_rows = token_rows.astype(jnp.float32) * jax.nn.silu(gate.astype(jnp.float32))
    scale_rows = lax.rsqrt(jnp.mean(gated_rows * gated_rows, axis=-1, keepdims=True) + EPS)
    return (gated_rows * scale_rows * out_gain).astype(jnp.bfloat16)


def solution(mesh):
    return jax.shard_map(
        per_device,
        mesh=mesh,
        in_specs=(
            P(("dp", "sp"), None),
            P(("dp", "sp"), None),
            P(("dp", "sp"), None),
            P(),
            P(None, "dp"),
            P(("dp", "sp"), None),
            P(),
        ),
        out_specs=P(("dp", "sp"), None),
        check_vma=False,
    )
```

profile of v0, /device:TPU:8, one launch (start us, length us, event | category | flops | bytes accessed | tf_op | source)
XLA Modules:
  0.0 278.0 jit_solution(5976931859334378445)
XLA Ops:
  8.4 11.7 %all-to-all-start.2 = ((bf16[32,128,64]{1,2,0:T(8,128)(2,1)}), bf16[32,128,64]{1,2,0:T(8,128)(2,1)S(1)}, u32[]{:S(2)}, u32[]{:S(2)}) async-start(bf16[32,128,64]{1,2,0:T(8,128)(2,1)} %broadcast_in_dim.7), calls=%async_computation.2 | async-start | bytes 1048576 | tf_op jit(solution)/shard_map/all_to_all | solution.py:22
  20.1 1.9 copy.26
  23.6 13.3 %all-to-all-done.2 = bf16[32,128,64]{1,2,0:T(8,128)(2,1)S(1)} async-done(((bf16[32,128,64]{1,2,0:T(8,128)(2,1)}), bf16[32,128,64]{1,2,0:T(8,128)(2,1)S(1)}, u32[]{:S(2)}, u32[]{:S(2)}) %all-to-all-start.2) | async-done | bytes 524320 | tf_op jit(solution)/shard_map/all_to_all | solution.py:22
  36.9 5.6 %all-to-all-start = ((bf16[128,32,192]{0,2,1:T(8,128)(2,1)}), bf16[128,32,192]{0,2,1:T(8,128)(2,1)S(1)}, u32[]{:S(2)}, u32[]{:S(2)}) async-start(bf16[128,32,192]{0,2,1:T(8,128)(2,1)} %pad_maximum_fusion), calls=%async_computation | async-start | bytes 3145728 | tf_op jit(solution)/shard_map/all_to_all | solution.py:85
  42.6 56.9 %all-gather.2.cloned.1.call-done = bf16[1024,8192]{1,0:T(8,128)(2,1)} async-done(((bf16[1024,1024]{1,0:T(8,128)(2,1)}), bf16[1024,8192]{1,0:T(8,128)(2,1)}) %all-gather.2.cloned.1.call-update) | async-done | bytes 16777232 | tf_op jit(solution)/shard_map/all_gather | solution.py:75
  99.5 8.2 %convolution_convert_fusion = bf16[128,8192]{1,0:T(8,128)(2,1)S(1)} fusion(bf16[1024,8192]{1,0:T(8,128)(2,1)} %all-gather.2.cloned.1.call-done, bf16[128,1024]{1,0:T(8,128)(2,1)S(1)} %copy-done.3, f32[1024]{0:T(1024)S(1)} %copy-done.8, f32[128]{0:T(128)S(1)} %add_rsqrt_fusion.1), kind=kOutput, calls=%fused_computation.16 | convolution fusion | flops 2149056512 | bytes 19141120 | tf_op jit(solution)/shard_map/dot_general | solution.py:73
  107.7 1.6 copy.39
  110.5 10.2 %all-to-all-start.1 = ((bf16[128,32,256]{2,0,1:T(8,128)(2,1)}), bf16[128,32,256]{2,0,1:T(8,128)(2,1)S(1)}, u32[]{:S(2)}, u32[]{:S(2)}) async-start(bf16[128,32,256]{2,0,1:T(8,128)(2,1)} %bitcast.86), calls=%async_computation.1 | async-start | bytes 4194304 | tf_op jit(solution)/shard_map/all_to_all | solution.py:86
  122.2 3.6 %copy.27 = bf16[32,128,192]{1,0,2:T(8,128)(2,1)} copy(bf16[32,128,192]{1,2,0:T(8,128)(2,1)} %bitcast.88) | data formatting | bytes 3145728 | tf_op jit(solution)/shard_map/all_to_all | solution.py:85
  125.7 3.7 %reshape.157 = bf16[8,512,1,192]{1,0,3,2:T(8,128)(2,1)} reshape(bf16[32,128,192]{1,0,2:T(8,128)(2,1)} %copy.27) | data formatting | bytes 3145728 | tf_op jit(solution)/shard_map/while/body/eval_jaxpr/reshape | solution.py:98
  129.5 3.1 %copy.30 = bf16[8,512,1,192]{1,3,2,0:T(8,128)(2,1)} copy(bf16[8,512,1,192]{1,0,3,2:T(8,128)(2,1)} %reshape.157) | data formatting | bytes 3145728 | tf_op jit(solution)/shard_map/while/body/eval_jaxpr/while | solution.py:99
  132.5 37.7 %all-to-all-done.1 = bf16[128,32,256]{2,0,1:T(8,128)(2,1)S(1)} async-done(((bf16[128,32,256]{2,0,1:T(8,128)(2,1)}), bf16[128,32,256]{2,0,1:T(8,128)(2,1)S(1)}, u32[]{:S(2)}, u32[]{:S(2)}) %all-to-all-start.1) | async-done | bytes 2097184 | tf_op jit(solution)/shard_map/all_to_all | solution.py:86
  171.6 2.7 fusion.35
  174.3 57.8 %while.17 = (s32[]{:T(128)}, bf16[8,512,1,128]{3,1,2,0:T(8,128)(2,1)S(1)}, bf16[8,512,1,192]{1,3,2,0:T(8,128)(2,1)}, bf16[4096,1,128]{2,0,1:T(8,128)(2,1)S(1)}, ...) while((s32[]{:T(128)}, bf16[8,512,1,128]{3,1,2,0:T(8,128)(2,1)S(1)}, ...), condition=%wide.region_4.5_spmd, body=%wide.region_1.4_spmd.sunk | while | flops 1359019008 | bytes 50014328 | solution.py:99
  179.3 2.2 fusion.53
  186.5 2.2 fusion.53
  193.7 2.2 fusion.53
  200.9 2.2 fusion.53
  208.2 2.2 fusion.53
  215.4 2.2 fusion.53
  222.6 2.2 fusion.53
  229.8 2.2 fusion.53
  233.1 6.3 %all-to-all-start.3 = ((bf16[32,128,128]{2,1,0:T(8,128)(2,1)}), bf16[32,128,128]{2,1,0:T(8,128)(2,1)S(1)}, u32[]{:S(2)}, u32[]{:S(2)}) async-start(bf16[32,128,128]{2,1,0:T(8,128)(2,1)} %bitcast.91), calls=%async_computation.3 | async-start | bytes 2097152 | tf_op jit(solution)/shard_map/all_to_all | solution.py:113
  240.1 27.4 %all-to-all-done.3 = bf16[32,128,128]{2,1,0:T(8,128)(2,1)S(1)} async-done(((bf16[32,128,128]{2,1,0:T(8,128)(2,1)}), bf16[32,128,128]{2,1,0:T(8,128)(2,1)S(1)}, u32[]{:S(2)}, u32[]{:S(2)}) %all-to-all-start.3) | async-done | bytes 1048608 | tf_op jit(solution)/shard_map/all_to_all | solution.py:113
  (89 shorter events, 52.3 us)
Async XLA Ops:
  6.5 0.8 copy-start.10
  6.5 93.0 %all-gather.2.cloned.1.call-start = ((), (), s32[]{:S(2)}) async-start(), calls=%async_computation.4 | async-start | bytes 18874368 | tf_op jit(solution)/shard_map/all_gather | solution.py:75
  8.4 28.5 %all-to-all-start.2 = ((bf16[32,128,64]{1,2,0:T(8,128)(2,1)}), bf16[32,128,64]{1,2,0:T(8,128)(2,1)S(1)}, u32[]{:S(2)}, u32[]{:S(2)}) async-start(bf16[32,128,64]{1,2,0:T(8,128)(2,1)} %broadcast_in_dim.7), calls=%async_computation.2 | async-start | bytes 1048576 | tf_op jit(solution)/shard_map/all_to_all | solution.py:22
  23.6 18.9 %copy-start.3 = (bf16[128,1024]{1,0:T(8,128)(2,1)S(1)}, bf16[128,1024]{1,0:T(8,128)(2,1)}, u32[]{:S(2)}) copy-start(bf16[128,1024]{1,0:T(8,128)(2,1)} %param.10) | copy-start | bytes 786436
  23.6 75.9 %copy-start.8 = (f32[1024]{0:T(1024)S(1)}, f32[1024]{0:T(1024)}, u32[]{:S(2)}) copy-start(f32[1024]{0:T(1024)} %param.12) | copy-start | bytes 12292
  36.9 70.8 %copy-start.2 = (bf16[32,128,64]{1,2,0:T(8,128)(2,1)}, bf16[32,128,64]{1,2,0:T(8,128)(2,1)S(1)}, u32[]{:S(2)}) copy-start(bf16[32,128,64]{1,2,0:T(8,128)(2,1)S(1)} %all-to-all-done.2) | copy-start | bytes 1572868
  36.9 72.4 %all-to-all-start = ((bf16[128,32,192]{0,2,1:T(8,128)(2,1)}), bf16[128,32,192]{0,2,1:T(8,128)(2,1)S(1)}, u32[]{:S(2)}, u32[]{:S(2)}) async-start(bf16[128,32,192]{0,2,1:T(8,128)(2,1)} %pad_maximum_fusion), calls=%async_computation | async-start | bytes 3145728 | tf_op jit(solution)/shard_map/all_to_all | solution.py:85
  109.3 1.2 copy-start.1
  110.5 59.8 %all-to-all-start.1 = ((bf16[128,32,256]{2,0,1:T(8,128)(2,1)}), bf16[128,32,256]{2,0,1:T(8,128)(2,1)S(1)}, u32[]{:S(2)}, u32[]{:S(2)}) async-start(bf16[128,32,256]{2,0,1:T(8,128)(2,1)} %bitcast.86), calls=%async_computation.1 | async-start | bytes 4194304 | tf_op jit(solution)/shard_map/all_to_all | solution.py:86
  170.2 1.3 copy-start
  171.6 2.7 copy-start.5
  178.0 1.3 copy-start.7
  185.2 1.3 copy-start.7
  192.4 1.3 copy-start.7
  199.7 1.3 copy-start.7
  206.9 1.3 copy-start.7
  214.1 1.3 copy-start.7
  221.3 1.3 copy-start.7
  228.6 1.3 copy-start.7
  232.1 1.0 copy-start.6
  232.1 7.3 %copy-start.4 = (bf16[128,4096]{1,0:T(8,128)(2,1)S(1)}, bf16[128,4096]{1,0:T(8,128)(2,1)}, u32[]{:S(2)}) copy-start(bf16[128,4096]{1,0:T(8,128)(2,1)} %param.14) | copy-start | bytes 3145732
  233.1 34.4 %all-to-all-start.3 = ((bf16[32,128,128]{2,1,0:T(8,128)(2,1)}), bf16[32,128,128]{2,1,0:T(8,128)(2,1)S(1)}, u32[]{:S(2)}, u32[]{:S(2)}) async-start(bf16[32,128,128]{2,1,0:T(8,128)(2,1)} %bitcast.91), calls=%async_computation.3 | async-start | bytes 2097152 | tf_op jit(solution)/shard_map/all_to_all | solution.py:113
  240.1 28.8 %copy-start.9 = (f32[4096]{0:T(1024)S(1)}, f32[4096]{0:T(1024)}, u32[]{:S(2)}) copy-start(f32[4096]{0:T(1024)} %param.15) | copy-start | bytes 49156
Sparse Core Ops, SparseCore 0:
  9.2 90.2 all-gather.1
where the time goes:
time: 279 us; the launch traced here: 278 us
  waiting for transfers between devices  136 us (49%)
  matrix products  47.9 us (17%)
  starting transfers between devices  33.8 us (12%)
  local copies, waits for them, and re-layouts  32.8 us (12%)
  other arithmetic  13.6 us (5%)
  between operations  13.6 us (5%)
    all_gather x1, waiting for transfers between devices, per_device(): lax.all_gather(kv_weight, 'dp', axis=1, tiled=True)  56.9 us
    all_to_all x1, waiting for transfers between devices, per_device(): lax.all_to_all(keyval, 'sp', split_axis=1, concat_axis=0, tiled=True)  37.7 us
    all_to_all x1, waiting for transfers between devices, per_device(): lax.all_to_all(heads_out, 'sp', split_axis=0, concat_axis=1, tiled=True)  27.4 us
    dot_general x8, matrix products, attend(): jnp.einsum('hqk,khd->qhd', weights, values, preferred_element_type=jnp.fl...  18 us
    all_to_all x1, waiting for transfers between devices, copy_for_each(): lax.all_to_all(jnp.broadcast_to(value[None], (length, *value.shape)), axi...  13.3 us
    all_to_all x1, starting transfers between devices, copy_for_each(): lax.all_to_all(jnp.broadcast_to(value[None], (length, *value.shape)), axi...  11.7 us
    dot_general x8, matrix products, attend(): jnp.einsum('qhr,kr->hqk', query_block[..., NOPE:], keys_rotated, preferre...  11.4 us
    dot_general x8, matrix products, attend(): jnp.einsum('qhd,khd->hqk', query_block[..., :NOPE], keys_plain, preferred...  10.3 us
  transfers between devices with their start and end apart: 5, of which 4 were waited for; matrix products, arithmetic and copies ran while one was open for 10% of the time, Pallas kernels for 0%

commit v1 on v0

--- a/solution.py
+++ b/solution.py
@@ -9,6 +9,27 @@
 VDIM = 128
 EPS = 1e-06
 THETA = 10000.0
+
+
+def gather_around(x, axis, dim):
+    devices, mine, rows = (lax.axis_size(axis), lax.axis_index(axis), x.shape[dim])
+    ahead = [(i, (i + 1) % devices) for i in range(devices)]
+    left = [(i, (i - 1) % devices) for i in range(devices)]
+    whole = jnp.zeros((*x.shape[:dim], devices * rows, *x.shape[dim + 1 :]), x.dtype)
+    whole = lax.dynamic_update_slice_in_dim(whole, x, mine * rows, axis=dim)
+    from_left = from_right = x
+    half = devices // 2
+    for hop in range(1, half + 1):
+        from_left = lax.ppermute(from_left, axis, ahead)
+        whole = lax.dynamic_update_slice_in_dim(
+            whole, from_left, (mine - hop) % devices * rows, axis=dim
+        )
+        if hop < devices - half:
+            from_right = lax.ppermute(from_right, axis, left)
+            whole = lax.dynamic_update_slice_in_dim(
+                whole, from_right, (mine + hop) % devices * rows, axis=dim
+            )
+    return whole
 
 
 def in_order(blocks, dim):
@@ -71,9 +92,7 @@
         widened * lax.rsqrt(jnp.mean(widened * widened, axis=-1, keepdims=True) + EPS) * latent_gain
     ).astype(jnp.bfloat16)
     keyval = jnp.dot(
-        normed,
-        lax.all_gather(kv_weight, "dp", axis=1, tiled=True),
-        preferred_element_type=jnp.float32,
+        normed, gather_around(kv_weight, "dp", 1), preferred_element_type=jnp.float32
     ).astype(jnp.bfloat16)
     head_queries = queries.reshape(own_tokens, HEADS, NOPE + ROPE)
     head_queries = jnp.concatenate(

time: 279 us -> 292 us (1.047)
  the two profiles are of different devices: /device:TPU:8 before, /device:TPU:14 now
where the time goes in v1:
time: 292 us; the launch traced here: 291 us
  waiting for transfers between devices  146 us (50%)
  local copies, waits for them, and re-layouts  48.8 us (17%)
  matrix products  42.2 us (14%)
  starting transfers between devices  38.6 us (13%)
  other arithmetic  14.3 us (5%)
    ppermute x4, waiting for transfers between devices, gather_around(): from_left = lax.ppermute(from_left, axis, ahead)  56.9 us
    all_to_all x1, waiting for transfers between devices, per_device(): lax.all_to_all(keyval, 'sp', split_axis=1, concat_axis=0, tiled=True)  40.5 us
    all_to_all x1, waiting for transfers between devices, per_device(): lax.all_to_all(heads_out, 'sp', split_axis=0, concat_axis=1, tiled=True)  27.6 us
    all_to_all x1, waiting for transfers between devices, per_device(): lax.all_to_all(head_queries, 'sp', split_axis=1, concat_axis=0, tiled=True)  19.3 us
    dot_general x8, matrix products, attend(): jnp.einsum('hqk,khd->qhd', weights, values, preferred_element_type=jnp.fl...  18 us
    all_to_all x1, starting transfers between devices, copy_for_each(): lax.all_to_all(jnp.broadcast_to(value[None], (length, *value.shape)), axi...  11.7 us
    dot_general x8, matrix products, attend(): jnp.einsum('qhr,kr->hqk', query_block[..., NOPE:], keys_rotated, preferre...  11.4 us
    dot_general x8, matrix products, attend(): jnp.einsum('qhd,khd->hqk', query_block[..., :NOPE], keys_plain, preferred...  10.3 us
  transfers between devices with their start and end apart: 11, of which 7 were waited for; matrix products, arithmetic and copies ran while one was open for 12% of the time, Pallas kernels for 0%

profile of v1, /device:TPU:14, one launch (start us, length us, event | category | flops | bytes accessed | tf_op | source)
XLA Modules:
  0.0 290.9 jit_solution(5706441281551759901)
XLA Ops:
  1.7 23.9 %collective-permute-done = bf16[1024,1024]{1,0:T(8,128)(2,1)S(1)} collective-permute-done((bf16[1024,1024]{1,0:T(8,128)(2,1)}, bf16[1024,1024]{1,0:T(8,128)(2,1)S(1)}, u32[]{:S(2)}, u32[]{:S(2)}) %collective-permute-start) | collective-permute-done | bytes 2097184 | tf_op jit(solution)/shard_map/ppermute | solution.py:23
  28.8 23.8 %collective-permute-done.2 = bf16[1024,1024]{1,0:T(8,128)(2,1)} collective-permute-done((bf16[1024,1024]{1,0:T(8,128)(2,1)S(1)}, bf16[1024,1024]{1,0:T(8,128)(2,1)}, u32[]{:S(2)}, u32[]{:S(2)}) %collective-permute-start.2) | collective-permute-done | bytes 2097184 | tf_op jit(solution)/shard_map/ppermute | solution.py:23
  54.4 11.7 %all-to-all-start.2 = ((bf16[32,128,64]{1,2,0:T(8,128)(2,1)}), bf16[32,128,64]{1,2,0:T(8,128)(2,1)S(1)}, u32[]{:S(2)}, u32[]{:S(2)}) async-start(bf16[32,128,64]{1,2,0:T(8,128)(2,1)} %broadcast_in_dim.10), calls=%async_computation.2 | async-start | bytes 1048576 | tf_op jit(solution)/shard_map/all_to_all | solution.py:43
  69.2 9.1 %collective-permute-done.4 = bf16[1024,1024]{1,0:T(8,128)(2,1)} collective-permute-done((bf16[1024,1024]{1,0:T(8,128)(2,1)}, bf16[1024,1024]{1,0:T(8,128)(2,1)}, u32[]{:S(2)}, u32[]{:S(2)}) %collective-permute-start.4) | collective-permute-done | bytes 2097184 | tf_op jit(solution)/shard_map/ppermute | solution.py:23
  82.4 9.9 %all-to-all-start = ((bf16[128,32,192]{0,2,1:T(8,128)(2,1)}), bf16[128,32,192]{0,2,1:T(8,128)(2,1)S(1)}, u32[]{:S(2)}, u32[]{:S(2)}) async-start(bf16[128,32,192]{0,2,1:T(8,128)(2,1)} %pad_maximum_fusion), calls=%async_computation | async-start | bytes 3145728 | tf_op jit(solution)/shard_map/all_to_all | solution.py:104
  107.4 2.5 convolution_convert_fusion
  111.5 19.3 %all-to-all-done = bf16[128,32,192]{0,2,1:T(8,128)(2,1)S(1)} async-done(((bf16[128,32,192]{0,2,1:T(8,128)(2,1)}), bf16[128,32,192]{0,2,1:T(8,128)(2,1)S(1)}, u32[]{:S(2)}, u32[]{:S(2)}) %all-to-all-start) | async-done | bytes 1572896 | tf_op jit(solution)/shard_map/all_to_all | solution.py:104
  131.9 6.2 %all-to-all-start.1 = ((bf16[128,32,256]{2,0,1:T(8,128)(2,1)}), bf16[128,32,256]{2,0,1:T(8,128)(2,1)S(1)}, u32[]{:S(2)}, u32[]{:S(2)}) async-start(bf16[128,32,256]{2,0,1:T(8,128)(2,1)} %bitcast.86), calls=%async_computation.1 | async-start | bytes 4194304 | tf_op jit(solution)/shard_map/all_to_all | solution.py:105
  139.7 3.6 %copy.27 = bf16[32,128,192]{1,0,2:T(8,128)(2,1)} copy(bf16[32,128,192]{1,2,0:T(8,128)(2,1)} %bitcast.88) | data formatting | bytes 3145728 | tf_op jit(solution)/shard_map/all_to_all | solution.py:104
  143.3 3.7 %reshape.157 = bf16[8,512,1,192]{1,0,3,2:T(8,128)(2,1)} reshape(bf16[32,128,192]{1,0,2:T(8,128)(2,1)} %copy.27) | data formatting | bytes 3145728 | tf_op jit(solution)/shard_map/while/body/eval_jaxpr/reshape | solution.py:117
  147.0 3.0 %copy.30 = bf16[8,512,1,192]{1,3,2,0:T(8,128)(2,1)} copy(bf16[8,512,1,192]{1,0,3,2:T(8,128)(2,1)} %reshape.157) | data formatting | bytes 3145728 | tf_op jit(solution)/shard_map/while/body/eval_jaxpr/while | solution.py:118
  150.0 40.5 %all-to-all-done.1 = bf16[128,32,256]{2,0,1:T(8,128)(2,1)S(1)} async-done(((bf16[128,32,256]{2,0,1:T(8,128)(2,1)}), bf16[128,32,256]{2,0,1:T(8,128)(2,1)S(1)}, u32[]{:S(2)}, u32[]{:S(2)}) %all-to-all-start.1) | async-done | bytes 2097184 | tf_op jit(solution)/shard_map/all_to_all | solution.py:105
  191.9 2.8 fusion.35
  194.7 57.8 %while.17 = (s32[]{:T(128)}, bf16[8,512,1,128]{3,1,2,0:T(8,128)(2,1)S(1)}, bf16[8,512,1,192]{1,3,2,0:T(8,128)(2,1)}, bf16[4096,1,128]{2,0,1:T(8,128)(2,1)S(1)}, ...) while((s32[]{:T(128)}, bf16[8,512,1,128]{3,1,2,0:T(8,128)(2,1)S(1)}, ...), condition=%wide.region_4.5_spmd, body=%wide.region_1.4_spmd.sunk | while | flops 1359019008 | bytes 50014320 | solution.py:118
  199.6 2.2 fusion.53
  206.8 2.2 fusion.53
  214.1 2.2 fusion.53
  221.3 2.2 fusion.53
  228.5 2.2 fusion.53
  235.7 2.2 fusion.53
  243.0 2.2 fusion.53
  250.2 2.2 fusion.53
  253.4 5.6 %all-to-all-start.3 = ((bf16[32,128,128]{2,1,0:T(8,128)(2,1)}), bf16[32,128,128]{2,1,0:T(8,128)(2,1)S(1)}, u32[]{:S(2)}, u32[]{:S(2)}) async-start(bf16[32,128,128]{2,1,0:T(8,128)(2,1)} %bitcast.91), calls=%async_computation.3 | async-start | bytes 2097152 | tf_op jit(solution)/shard_map/all_to_all | solution.py:132
  259.7 27.6 %all-to-all-done.3 = bf16[32,128,128]{2,1,0:T(8,128)(2,1)S(1)} async-done(((bf16[32,128,128]{2,1,0:T(8,128)(2,1)}), bf16[32,128,128]{2,1,0:T(8,128)(2,1)S(1)}, u32[]{:S(2)}, u32[]{:S(2)}) %all-to-all-start.3) | async-done | bytes 1048608 | tf_op jit(solution)/shard_map/all_to_all | solution.py:132
  (113 shorter events, 78.9 us)
Async XLA Ops:
  0.0 25.7 %collective-permute-start = (bf16[1024,1024]{1,0:T(8,128)(2,1)}, bf16[1024,1024]{1,0:T(8,128)(2,1)S(1)}, u32[]{:S(2)}, u32[]{:S(2)}) collective-permute-start(bf16[1024,1024]{1,0:T(8,128)(2,1)} %param.13), channel_id=1, source_target_pairs={{0,1},{1,2},{2,3},{3,4},{4,5},{5,6},{6,7},{7,0},{8,9},{9,10},{10,1... | collective-permute-start | bytes 6291464 | tf_op jit(solution)/shard_map/ppermute | solution.py:23
  0.0 27.0 %collective-permute-start.1 = (bf16[1024,1024]{1,0:T(8,128)(2,1)}, bf16[1024,1024]{1,0:T(8,128)(2,1)}, u32[]{:S(2)}, u32[]{:S(2)}) collective-permute-start(bf16[1024,1024]{1,0:T(8,128)(2,1)} %param.13), channel_id=1, source_target_pairs={{0,7},{1,0},{2,1},{3,2},{4,3},{5,4},{6,5},{7,6},{8,15},{9,8},{10,9... | collective-permute-start | bytes 6291464 | tf_op jit(solution)/shard_map/ppermute | solution.py:28
  25.7 1.3 copy-start.4
  27.0 25.6 %collective-permute-start.2 = (bf16[1024,1024]{1,0:T(8,128)(2,1)S(1)}, bf16[1024,1024]{1,0:T(8,128)(2,1)}, u32[]{:S(2)}, u32[]{:S(2)}) collective-permute-start(bf16[1024,1024]{1,0:T(8,128)(2,1)S(1)} %collective-permute-done), channel_id=1, source_target_pairs={{0,1},{1,2},{2,3},{3,4},{4,5},{5,6},{6,7},{7,0},{8,9},{9,10},{10,1... | collective-permute-start | bytes 6291464 | tf_op jit(solution)/shard_map/ppermute | solution.py:23
  27.0 41.0 %collective-permute-start.3 = (bf16[1024,1024]{1,0:T(8,128)(2,1)}, bf16[1024,1024]{1,0:T(8,128)(2,1)}, u32[]{:S(2)}, u32[]{:S(2)}) collective-permute-start(bf16[1024,1024]{1,0:T(8,128)(2,1)} %collective-permute-done.1), channel_id=1, source_target_pairs={{0,7},{1,0},{2,1},{3,2},{4,3},{5,4},{6,5},{7,6},{8,15},{9,8},{10,9... | collective-permute-start | bytes 6291464 | tf_op jit(solution)/shard_map/ppermute | solution.py:28
  52.6 25.8 %collective-permute-start.4 = (bf16[1024,1024]{1,0:T(8,128)(2,1)}, bf16[1024,1024]{1,0:T(8,128)(2,1)}, u32[]{:S(2)}, u32[]{:S(2)}) collective-permute-start(bf16[1024,1024]{1,0:T(8,128)(2,1)} %collective-permute-done.2), channel_id=1, source_target_pairs={{0,1},{1,2},{2,3},{3,4},{4,5},{5,6},{6,7},{7,0},{8,9},{9,10},{10,1... | collective-permute-start | bytes 6291464 | tf_op jit(solution)/shard_map/ppermute | solution.py:23
  54.4 28.0 %all-to-all-start.2 = ((bf16[32,128,64]{1,2,0:T(8,128)(2,1)}), bf16[32,128,64]{1,2,0:T(8,128)(2,1)S(1)}, u32[]{:S(2)}, u32[]{:S(2)}) async-start(bf16[32,128,64]{1,2,0:T(8,128)(2,1)} %broadcast_in_dim.10), calls=%async_computation.2 | async-start | bytes 1048576 | tf_op jit(solution)/shard_map/all_to_all | solution.py:43
  68.0 35.6 %collective-permute-start.5 = (bf16[1024,1024]{1,0:T(8,128)(2,1)}, bf16[1024,1024]{1,0:T(8,128)(2,1)}, u32[]{:S(2)}, u32[]{:S(2)}) collective-permute-start(bf16[1024,1024]{1,0:T(8,128)(2,1)} %collective-permute-done.3), channel_id=1, source_target_pairs={{0,7},{1,0},{2,1},{3,2},{4,3},{5,4},{6,5},{7,6},{8,15},{9,8},{10,9... | collective-permute-start | bytes 6291464 | tf_op jit(solution)/shard_map/ppermute | solution.py:28
  78.3 27.2 %collective-permute-start.6 = (bf16[1024,1024]{1,0:T(8,128)(2,1)}, bf16[1024,1024]{1,0:T(8,128)(2,1)}, u32[]{:S(2)}, u32[]{:S(2)}) collective-permute-start(bf16[1024,1024]{1,0:T(8,128)(2,1)} %collective-permute-done.4), channel_id=1, source_target_pairs={{0,1},{1,2},{2,3},{3,4},{4,5},{5,6},{6,7},{7,0},{8,9},{9,10},{10,1... | collective-permute-start | bytes 6291464 | tf_op jit(solution)/shard_map/ppermute | solution.py:23
  80.5 12.0 %copy-start.6 = (bf16[128,1024]{1,0:T(8,128)(2,1)S(1)}, bf16[128,1024]{1,0:T(8,128)(2,1)}, u32[]{:S(2)}) copy-start(bf16[128,1024]{1,0:T(8,128)(2,1)} %param.10) | copy-start | bytes 786436
  82.4 11.8 %copy-start.2 = (bf16[32,128,64]{1,2,0:T(8,128)(2,1)}, bf16[32,128,64]{1,2,0:T(8,128)(2,1)S(1)}, u32[]{:S(2)}) copy-start(bf16[32,128,64]{1,2,0:T(8,128)(2,1)S(1)} %all-to-all-done.2) | copy-start | bytes 1572868
  82.4 48.4 %all-to-all-start = ((bf16[128,32,192]{0,2,1:T(8,128)(2,1)}), bf16[128,32,192]{0,2,1:T(8,128)(2,1)S(1)}, u32[]{:S(2)}, u32[]{:S(2)}) async-start(bf16[128,32,192]{0,2,1:T(8,128)(2,1)} %pad_maximum_fusion), calls=%async_computation | async-start | bytes 3145728 | tf_op jit(solution)/shard_map/all_to_all | solution.py:104
  92.6 1.7 copy-start.3
  94.3 1.6 copy-start.5
  105.5 1.9 copy-start.11
  131.9 58.7 %all-to-all-start.1 = ((bf16[128,32,256]{2,0,1:T(8,128)(2,1)}), bf16[128,32,256]{2,0,1:T(8,128)(2,1)S(1)}, u32[]{:S(2)}, u32[]{:S(2)}) async-start(bf16[128,32,256]{2,0,1:T(8,128)(2,1)} %bitcast.86), calls=%async_computation.1 | async-start | bytes 4194304 | tf_op jit(solution)/shard_map/all_to_all | solution.py:105
  190.6 1.3 copy-start
  191.9 2.8 copy-start.8
  212.8 1.3 copy-start.10
  220.0 1.3 copy-start.10
  227.2 1.3 copy-start.10
  252.5 6.6 %copy-start.7 = (bf16[128,4096]{1,0:T(8,128)(2,1)S(1)}, bf16[128,4096]{1,0:T(8,128)(2,1)}, u32[]{:S(2)}) copy-start(bf16[128,4096]{1,0:T(8,128)(2,1)} %param.14) | copy-start | bytes 3145732
  253.4 33.9 %all-to-all-start.3 = ((bf16[32,128,128]{2,1,0:T(8,128)(2,1)}), bf16[32,128,128]{2,1,0:T(8,128)(2,1)S(1)}, u32[]{:S(2)}, u32[]{:S(2)}) async-start(bf16[32,128,128]{2,1,0:T(8,128)(2,1)} %bitcast.91), calls=%async_computation.3 | async-start | bytes 2097152 | tf_op jit(solution)/shard_map/all_to_all | solution.py:132
  259.7 29.0 %copy-start.12 = (f32[4096]{0:T(1024)S(1)}, f32[4096]{0:T(1024)}, u32[]{:S(2)}) copy-start(f32[4096]{0:T(1024)} %param.15) | copy-start | bytes 49156
  (7 other events, 8.5 us)
